TPU v7x, 256 devices: a 4x2x16 block of a 4x16x16 slice. The times are simulated.
256 devices in a mesh: grp: 2 (over y), fs: 16 (over z), tp: 8 (over x, core).
Axes of the slice: x: 4, y: 2, z: 16, core: 2. Of those that a mesh axis runs over, the one named last changes fastest.
The devices are a block of a 4x16x16 slice.
Arguments:
- tokens: bfloat16 [32768, 2048], P(('grp', 'fs')), parts along dimension 0, may hold values from -1300 to 1300
- norm_gain: bfloat16 [2048], replicated, may hold values from 0.099609375 to 1.8984375
- gate_weight: bfloat16 [2048, 5120], P('fs', 'tp'), may hold values from -0.125 to 0.125
- up_weight: bfloat16 [2048, 5120], P('fs', 'tp'), may hold values from -0.125 to 0.125
- down_weight: bfloat16 [5120, 2048], P('tp', 'fs'), may hold values from -0.078125 to 0.078125
Outputs:
- mixed: bfloat16 [32768, 2048], P(('grp', 'fs', 'tp')), parts along dimension 0
There are 2 independent parts, one for each index of `grp`. A program takes and returns all parts, laid end to end along the dimension named above; an argument that names none is the same for every part. Nothing has to cross between parts.
All inputs are finite; a program needn't handle non-finite values.
Results may differ from a plain program's by a relative error of at most 0.013.
Values may be sent and summed in bfloat16 or wider, within the bound.
No kernel may reach another device: no remote copies, remote signals or barrier semaphores. Data moves between devices by JAX's collectives and lax.ppermute only.
A program may use at most 64 MiB of HBM per device.

v0:
```python
import jax
import jax.numpy as jnp
from jax import lax
from jax.sharding import PartitionSpec as P

EPSILON = 1e-06


def side_by_side(arrays, axis, dim, along):
    widths = [a.shape[along] for a in arrays]
    both = jnp.concatenate(arrays, axis=along)
    result = lax.all_gather(both, axis, axis=dim, tiled=True)
    return tuple(jnp.split(result, [sum(widths[:k]) for k in range(1, len(widths))], axis=along))


def normalize(tokens, norm_gain):
    as_float = tokens.astype(jnp.float32)
    scale = lax.rsqrt(jnp.mean(as_float * as_float, axis=-1, keepdims=True) + EPSILON)
    return (as_float * scale * norm_gain.astype(jnp.float32)).astype(jnp.bfloat16)


def rounded(values):
    return lax.optimization_barrier(values.astype(jnp.bfloat16)).astype(jnp.float32)


def on_device(tokens, norm_gain, gate_weight, up_weight, down_weight):
    normed = normalize(tokens, norm_gain)
    down_whole = lax.all_gather(down_weight, "fs", axis=1, tiled=True)
    gate_whole, up_whole = side_by_side((gate_weight, up_weight), "fs", 0, 1)
    gate_acts = jnp.dot(normed, gate_whole, preferred_element_type=jnp.float32)
    up_acts = jnp.dot(normed, up_whole, preferred_element_type=jnp.float32)
    hidden = (jax.nn.silu(gate_acts) * up_acts).astype(jnp.bfloat16)
    return lax.psum_scatter(
        rounded(jnp.dot(hidden, down_whole, preferred_element_type=jnp.float32)).astype(
            jnp.bfloat16
        ),
        "tp",
        scatter_dimension=0,
        tiled=True,
    )


def solution(mesh):
    return jax.shard_map(
        on_device,
        mesh=mesh,
        in_specs=(P(("grp", "fs"), None), P(), P("fs", "tp"), P("fs", "tp"), P("tp", "fs")),
        out_specs=P(("grp", "fs", "tp"), None),
        check_vma=False,
    )
```

profile of v0, /device:TPU:40, one launch (start us, length us, event | category | flops | bytes accessed | tf_op | source)
XLA Modules:
  0.0 240.0 jit_solution(12156880815646767167)
XLA Ops:
  6.5 0.0 all-gather.3.cloned.1.call-start
  6.6 1.7 pad_maximum_fusion
  8.3 0.1 all-gather.3.cloned.1.call-update
  8.4 0.1 all-gather.5.cloned.1.call-start
  8.4 0.7 all-gather.5.cloned.1.call-update
  9.2 0.1 reduce-scatter.2.cloned.1.call-start
  9.2 0.7 convert_element_type.18
  9.9 3.1 %fusion = f32[1024]{0:T(1024)S(1)} fusion(bf16[1024,2048]{1,0:T(8,128)(2,1)} %param.5), kind=kLoop, calls=%fused_computation.2 | loop fusion | flops 6290432 | bytes 4198400 | tf_op jit(solution)/shard_map/reduce_sum | solution.py:18
  13.0 88.4 %all-gather.3.cloned.1.call-done = bf16[2048,1280]{1,0:T(8,128)(2,1)} async-done(((bf16[128,1280]{1,0:T(8,128)(2,1)}), bf16[2048,1280]{1,0:T(8,128)(2,1)}) %all-gather.3.cloned.1.call-update) | async-done | bytes 5242896 | tf_op jit(solution)/shard_map/all_gather | solution.py:12
  101.4 6.3 %fusion.3 = f32[1024,640]{1,0:T(8,128)S(1)} fusion(bf16[2048,1280]{1,0:T(8,128)(2,1)} %all-gather.3.cloned.1.call-done, bf16[1024,2048]{1,0:T(8,128)(2,1)} %param.5, f32[2048]{0:T(1024)S(1)} %convert_element_type.18, f32[1024]{0:T(1024)S(1)} %add_rsqrt_fusion), kind=kOutput, calls=%fused_computation.6 | convolution fusion | flops 2692743168 | bytes 9449472 | tf_op jit(solution)/shard_map/dot_general | solution.py:31
  107.7 72.3 %all-gather.5.cloned.1.call-done = bf16[640,2048]{1,0:T(8,128)(2,1)} async-done(((bf16[640,128]{1,0:T(8,128)(2,1)}), bf16[640,2048]{1,0:T(8,128)(2,1)}) %all-gather.5.cloned.1.call-update) | async-done | bytes 2621456 | tf_op jit(solution)/shard_map/all_gather | solution.py:28
  180.0 12.9 %convolution_convert_fusion = bf16[1024,2048]{1,0:T(8,128)(2,1)} fusion(bf16[640,2048]{1,0:T(8,128)(2,1)} %all-gather.5.cloned.1.call-done, f32[1024,640]{1,0:T(8,128)S(1)} %fusion.3, bf16[2048,1280]{1,0:T(8,128)(2,1)} %all-gather.3.cloned.1.call-done, bf16[1024,2048]{1,0:T(8,128)(2,1)} %param.5, f32[2048]{0:T(1024)S(1)} %convert_element_type.18, ...), kind=kOutput, calls=%fused_computation.5 | convolution fusion | flops 5383127040 | bytes 16265216 | tf_op jit(solution)/shard_map/dot_general | solution.py:34
  192.9 0.1 reduce-scatter.2.cloned.1.call-update
  192.9 40.5 %reduce-scatter.2.cloned.1.call-done = bf16[128,2048]{1,0:T(8,128)(2,1)} async-done(((bf16[1024,2048]{1,0:T(8,128)(2,1)}), bf16[128,2048]{1,0:T(8,128)(2,1)}) %reduce-scatter.2.cloned.1.call-update) | async-done | bytes 524304 | tf_op jit(solution)/shard_map/reduce_scatter | solution.py:33
  (1 shorter events, 0.0 us)
Async XLA Ops:
  6.5 94.9 %all-gather.3.cloned.1.call-start = ((), (), s32[]{:S(2)}) async-start(), calls=%async_computation.1 | async-start | bytes 5570560 | tf_op jit(solution)/shard_map/all_gather | solution.py:12
  8.4 171.7 %all-gather.5.cloned.1.call-start = ((), (), s32[]{:S(2)}) async-start(), calls=%async_computation.2 | async-start | bytes 2785280 | tf_op jit(solution)/shard_map/all_gather | solution.py:28
  9.2 224.2 %reduce-scatter.2.cloned.1.call-start = ((), (), s32[]{:S(2)}) async-start(), calls=%async_computation.3 | async-start | bytes 4718592 | tf_op jit(solution)/shard_map/reduce_scatter | solution.py:33
Sparse Core Ops, SparseCore 0:
  9.1 92.2 all-gather.2
  103.2 76.7 all-gather.4
  193.0 40.3 reduce-scatter.1
where the time goes:
time: 240 us
  waiting for transfers between devices  202 us (84%)
  matrix products  19.1 us (8%)
  between operations  13.1 us (5%)
  other arithmetic  5.51 us (2%)
    all_gather x1, waiting for transfers between devices, side_by_side(): result = lax.all_gather(both, axis, axis=dim, tiled=True)  88.4 us
    all_gather x1, waiting for transfers between devices, on_device(): down_whole = lax.all_gather(down_weight, 'fs', axis=1, tiled=True)  72.3 us
    reduce_scatter x1, waiting for transfers between devices, on_device(): lax.psum_scatter(rounded(jnp.dot(hidden, down_whole, preferred_element_ty...  40.5 us
    dot_general x1, matrix products, on_device(): jnp.dot(hidden, down_whole, preferred_element_type=jnp.float32)  12.9 us
    dot_general x1, matrix products, on_device(): up_acts = jnp.dot(normed, up_whole, preferred_element_type=jnp.float32)  6.29 us
  transfers between devices with their start and end apart: 3, of which 3 were waited for; matrix products, arithmetic and copies ran while one was open for 4% of the time, Pallas kernels for 0%

commit v1 on v0

--- a/solution.py
+++ b/solution.py
@@ -4,6 +4,19 @@
 from jax.sharding import PartitionSpec as P
 
 EPSILON = 1e-06
+
+
+def ring_gather(x, axis, dim):
+    ways = lax.axis_size(axis)
+    up = [(d, (d + 1) % ways) for d in range(ways)]
+    down = [(d, (d - 1) % ways) for d in range(ways)]
+    earlier, later = ([x], [x])
+    for _ in range(ways // 2):
+        earlier.append(lax.ppermute(earlier[-1], axis, up))
+    for _ in range((ways - 1) // 2):
+        later.append(lax.ppermute(later[-1], axis, down))
+    line = jnp.concatenate([*earlier[::-1], *later[1:]], axis=dim)
+    return jnp.roll(line, (lax.axis_index(axis) - ways // 2) * x.shape[dim], axis=dim)
 
 
 def side_by_side(arrays, axis, dim, along):
@@ -25,7 +38,7 @@
 
 def on_device(tokens, norm_gain, gate_weight, up_weight, down_weight):
     normed = normalize(tokens, norm_gain)
-    down_whole = lax.all_gather(down_weight, "fs", axis=1, tiled=True)
+    down_whole = ring_gather(down_weight, "fs", 1)
     gate_whole, up_whole = side_by_side((gate_weight, up_weight), "fs", 0, 1)
     gate_acts = jnp.dot(normed, gate_whole, preferred_element_type=jnp.float32)
     up_acts = jnp.dot(normed, up_whole, preferred_element_type=jnp.float32)

time: 240 us -> 196 us (0.82)
  waiting for transfers between devices: 202 us -> 105 us
  starting transfers between devices: 0.13 us -> 28.5 us
  local copies, waits for them, and re-layouts: 0 us -> 22.6 us
    all_gather x1, waiting for transfers between devices: 88.4 us -> 0.01 us  [side_by_side(): result = lax.all_gather(both, axis, axis=dim, tiled=True)]
    all_gather x1 -> x0, waiting for transfers between devices: 72.3 us -> none  [on_device(): down_whole = lax.all_gather(down_weight, 'fs', axis=1, tiled=True)]
    ppermute x0 -> x15, waiting for transfers between devices: none -> 66.6 us  [the longest x8 60.2 us: ring_gather(): earlier.append(lax.ppermute(earlier[-1], axis, up))]
    ppermute x0 -> x15, starting transfers between devices: none -> 28.4 us  [the longest x7 24.8 us: ring_gather(): later.append(lax.ppermute(later[-1], axis, down))]
    unnamed x0 -> x33, local copies, waits for them, and re-layouts: none -> 21.9 us
  transfers between devices with their start and end apart: 3 -> 17, of which waited for: 3 -> 14; matrix products, arithmetic and copies ran while one was open for 4% -> 13% of each run, Pallas kernels for 0% -> 0%
where the time goes in v1:
time: 196 us
  waiting for transfers between devices  105 us (54%)
  starting transfers between devices  28.5 us (15%)
  local copies, waits for them, and re-layouts  22.6 us (12%)
  matrix products  21.1 us (11%)
  between operations  13.5 us (7%)
  other arithmetic  5.58 us (3%)
    ppermute x8, waiting for transfers between devices, ring_gather(): earlier.append(lax.ppermute(earlier[-1], axis, up))  60.2 us
    reduce_scatter x1, waiting for transfers between devices, on_device(): lax.psum_scatter(rounded(jnp.dot(hidden, down_whole, preferred_element_ty...  38.1 us
    ppermute x7, starting transfers between devices, ring_gather(): later.append(lax.ppermute(later[-1], axis, down))  24.8 us
    unnamed x33, local copies, waits for them, and re-layouts  21.9 us
    dot_general x1, matrix products, on_device(): jnp.dot(hidden, down_whole, preferred_element_type=jnp.float32)  13.1 us
    dot_general x1, matrix products, on_device(): up_acts = jnp.dot(normed, up_whole, preferred_element_type=jnp.float32)  7.94 us
    ppermute x7, waiting for transfers between devices, ring_gather(): later.append(lax.ppermute(later[-1], axis, down))  6.44 us
  transfers between devices with their start and end apart: 17, of which 14 were waited for; matrix products, arithmetic and copies ran while one was open for 13% of the time, Pallas kernels for 0%

profile of v1, /device:TPU:40, one launch (start us, length us, event | category | flops | bytes accessed | tf_op | source)
XLA Modules:
  0.0 196.1 jit_solution(2840100580070030740)
XLA Ops:
  6.6 1.8 pad_maximum_fusion
  8.5 2.9 %collective-permute-start = (bf16[640,128]{1,0:T(8,128)(2,1)}, bf16[640,128]{1,0:T(8,128)(2,1)S(1)}, u32[]{:S(2)}, u32[]{:S(2)}) collective-permute-start(bf16[640,128]{1,0:T(8,128)(2,1)} %param.9), channel_id=1, source_target_pairs={{0,8},{8,16},{16,24},{24,32},{32,40},{40,48},{48,56},{56,64},{64,7... | collective-permute-start | bytes 491528 | tf_op jit(solution)/shard_map/ppermute | solution.py:15
  11.4 24.1 %collective-permute-done = bf16[640,128]{1,0:T(8,128)(2,1)S(1)} collective-permute-done((bf16[640,128]{1,0:T(8,128)(2,1)}, bf16[640,128]{1,0:T(8,128)(2,1)S(1)}, u32[]{:S(2)}, u32[]{:S(2)}) %collective-permute-start) | collective-permute-done | bytes 163872 | tf_op jit(solution)/shard_map/ppermute | solution.py:15
  35.5 3.2 %collective-permute-start.8 = (bf16[640,128]{1,0:T(8,128)(2,1)}, bf16[640,128]{1,0:T(8,128)(2,1)S(1)}, u32[]{:S(2)}, u32[]{:S(2)}) collective-permute-start(bf16[640,128]{1,0:T(8,128)(2,1)} %param.9), channel_id=1, source_target_pairs={{0,120},{8,0},{16,8},{24,16},{32,24},{40,32},{48,40},{56,48},{64,5... | collective-permute-start | bytes 491528 | tf_op jit(solution)/shard_map/ppermute | solution.py:17
  38.7 5.0 %collective-permute-done.1 = bf16[640,128]{1,0:T(8,128)(2,1)S(1)} collective-permute-done((bf16[640,128]{1,0:T(8,128)(2,1)S(1)}, bf16[640,128]{1,0:T(8,128)(2,1)S(1)}, u32[]{:S(2)}, u32[]{:S(2)}) %collective-permute-start.1) | collective-permute-done | bytes 163872 | tf_op jit(solution)/shard_map/ppermute | solution.py:15
  43.7 0.7 collective-permute-start.2
  45.0 3.6 %collective-permute-start.9 = (bf16[640,128]{1,0:T(8,128)(2,1)S(1)}, bf16[640,128]{1,0:T(8,128)(2,1)S(1)}, u32[]{:S(2)}, u32[]{:S(2)}) collective-permute-start(bf16[640,128]{1,0:T(8,128)(2,1)S(1)} %collective-permute-done.8), channel_id=1, source_target_pairs={{0,120},{8,0},{16,8},{24,16},{32,24},{40,32},{48,40},{56,48},{64,5... | collective-permute-start | bytes 491528 | tf_op jit(solution)/shard_map/ppermute | solution.py:17
  48.6 5.6 %collective-permute-done.2 = bf16[640,128]{1,0:T(8,128)(2,1)S(1)} collective-permute-done((bf16[640,128]{1,0:T(8,128)(2,1)S(1)}, bf16[640,128]{1,0:T(8,128)(2,1)S(1)}, u32[]{:S(2)}, u32[]{:S(2)}) %collective-permute-start.2) | collective-permute-done | bytes 163872 | tf_op jit(solution)/shard_map/ppermute | solution.py:15
  54.2 1.1 collective-permute-done.9
  55.3 3.7 %collective-permute-start.10 = (bf16[640,128]{1,0:T(8,128)(2,1)S(1)}, bf16[640,128]{1,0:T(8,128)(2,1)S(1)}, u32[]{:S(2)}, u32[]{:S(2)}) collective-permute-start(bf16[640,128]{1,0:T(8,128)(2,1)S(1)} %collective-permute-done.9), channel_id=1, source_target_pairs={{0,120},{8,0},{16,8},{24,16},{32,24},{40,32},{48,40},{56,48},{64,5... | collective-permute-start | bytes 491528 | tf_op jit(solution)/shard_map/ppermute | solution.py:17
  59.0 5.7 %collective-permute-done.3 = bf16[640,128]{1,0:T(8,128)(2,1)S(1)} collective-permute-done((bf16[640,128]{1,0:T(8,128)(2,1)S(1)}, bf16[640,128]{1,0:T(8,128)(2,1)S(1)}, u32[]{:S(2)}, u32[]{:S(2)}) %collective-permute-start.3) | collective-permute-done | bytes 163872 | tf_op jit(solution)/shard_map/ppermute | solution.py:15
  64.6 1.0 collective-permute-done.10
  65.7 3.7 %collective-permute-start.11 = (bf16[640,128]{1,0:T(8,128)(2,1)S(1)}, bf16[640,128]{1,0:T(8,128)(2,1)S(1)}, u32[]{:S(2)}, u32[]{:S(2)}) collective-permute-start(bf16[640,128]{1,0:T(8,128)(2,1)S(1)} %collective-permute-done.10), channel_id=1, source_target_pairs={{0,120},{8,0},{16,8},{24,16},{32,24},{40,32},{48,40},{56,48},{64,5... | collective-permute-start | bytes 491528 | tf_op jit(solution)/shard_map/ppermute | solution.py:17
  69.3 5.9 %collective-permute-done.4 = bf16[640,128]{1,0:T(8,128)(2,1)S(1)} collective-permute-done((bf16[640,128]{1,0:T(8,128)(2,1)S(1)}, bf16[640,128]{1,0:T(8,128)(2,1)S(1)}, u32[]{:S(2)}, u32[]{:S(2)}) %collective-permute-start.4) | collective-permute-done | bytes 163872 | tf_op jit(solution)/shard_map/ppermute | solution.py:15
  75.8 3.7 %collective-permute-start.12 = (bf16[640,128]{1,0:T(8,128)(2,1)S(1)}, bf16[640,128]{1,0:T(8,128)(2,1)S(1)}, u32[]{:S(2)}, u32[]{:S(2)}) collective-permute-start(bf16[640,128]{1,0:T(8,128)(2,1)S(1)} %collective-permute-done.11), channel_id=1, source_target_pairs={{0,120},{8,0},{16,8},{24,16},{32,24},{40,32},{48,40},{56,48},{64,5... | collective-permute-start | bytes 491528 | tf_op jit(solution)/shard_map/ppermute | solution.py:17
  79.5 6.7 %collective-permute-done.5 = bf16[640,128]{1,0:T(8,128)(2,1)S(1)} collective-permute-done((bf16[640,128]{1,0:T(8,128)(2,1)S(1)}, bf16[640,128]{1,0:T(8,128)(2,1)S(1)}, u32[]{:S(2)}, u32[]{:S(2)}) %collective-permute-start.5) | collective-permute-done | bytes 163872 | tf_op jit(solution)/shard_map/ppermute | solution.py:15
  86.2 3.1 %fusion = f32[1024]{0:T(1024)S(1)} fusion(bf16[1024,2048]{1,0:T(8,128)(2,1)} %param.5), kind=kLoop, calls=%fused_computation.2 | loop fusion | flops 6290432 | bytes 4198400 | tf_op jit(solution)/shard_map/reduce_sum | solution.py:31
  90.0 3.2 %collective-permute-start.13 = (bf16[640,128]{1,0:T(8,128)(2,1)S(1)}, bf16[640,128]{1,0:T(8,128)(2,1)S(1)}, u32[]{:S(2)}, u32[]{:S(2)}) collective-permute-start(bf16[640,128]{1,0:T(8,128)(2,1)S(1)} %collective-permute-done.12), channel_id=1, source_target_pairs={{0,120},{8,0},{16,8},{24,16},{32,24},{40,32},{48,40},{56,48},{64,5... | collective-permute-start | bytes 491528 | tf_op jit(solution)/shard_map/ppermute | solution.py:17
  93.3 4.2 %collective-permute-done.6 = bf16[640,128]{1,0:T(8,128)(2,1)S(1)} collective-permute-done((bf16[640,128]{1,0:T(8,128)(2,1)S(1)}, bf16[640,128]{1,0:T(8,128)(2,1)S(1)}, u32[]{:S(2)}, u32[]{:S(2)}) %collective-permute-start.6) | collective-permute-done | bytes 163872 | tf_op jit(solution)/shard_map/ppermute | solution.py:15
  97.5 3.2 %collective-permute-done.13 = bf16[640,128]{1,0:T(8,128)(2,1)S(1)} collective-permute-done((bf16[640,128]{1,0:T(8,128)(2,1)S(1)}, bf16[640,128]{1,0:T(8,128)(2,1)S(1)}, u32[]{:S(2)}, u32[]{:S(2)}) %collective-permute-start.13) | collective-permute-done | bytes 163872 | tf_op jit(solution)/shard_map/ppermute | solution.py:17
  100.6 3.7 %collective-permute-start.14 = (bf16[640,128]{1,0:T(8,128)(2,1)S(1)}, bf16[640,128]{1,0:T(8,128)(2,1)S(1)}, u32[]{:S(2)}, u32[]{:S(2)}) collective-permute-start(bf16[640,128]{1,0:T(8,128)(2,1)S(1)} %collective-permute-done.13), channel_id=1, source_target_pairs={{0,120},{8,0},{16,8},{24,16},{32,24},{40,32},{48,40},{56,48},{64,5... | collective-permute-start | bytes 491528 | tf_op jit(solution)/shard_map/ppermute | solution.py:17
  104.3 3.0 %collective-permute-done.7 = bf16[640,128]{1,0:T(8,128)(2,1)S(1)} collective-permute-done((bf16[640,128]{1,0:T(8,128)(2,1)S(1)}, bf16[640,128]{1,0:T(8,128)(2,1)S(1)}, u32[]{:S(2)}, u32[]{:S(2)}) %collective-permute-start.7) | collective-permute-done | bytes 163872 | tf_op jit(solution)/shard_map/ppermute | solution.py:15
  108.0 0.7 constant_dynamic-update-slice_fusion.30
  108.8 0.7 constant_dynamic-update-slice_fusion.29
  109.5 0.7 constant_dynamic-update-slice_fusion.28
  110.2 0.7 constant_dynamic-update-slice_fusion.27
  110.9 0.7 constant_dynamic-update-slice_fusion.26
  111.6 0.7 constant_dynamic-update-slice_fusion.25
  113.0 0.7 constant_dynamic-update-slice_fusion.23
  114.4 0.7 constant_dynamic-update-slice_fusion.21
  115.1 0.7 constant_dynamic-update-slice_fusion.20
  115.9 0.7 constant_dynamic-update-slice_fusion.19
  118.0 0.7 constant_dynamic-update-slice_fusion.16
  120.0 0.7 constant_dynamic-update-slice_fusion.13
  120.7 0.7 constant_dynamic-update-slice_fusion.12
  122.1 0.7 constant_dynamic-update-slice_fusion.10
  122.8 0.7 constant_dynamic-update-slice_fusion.9
  123.6 0.7 constant_dynamic-update-slice_fusion.8
  124.3 0.7 constant_dynamic-update-slice_fusion.7
  125.0 0.7 constant_dynamic-update-slice_fusion.6
  125.7 0.8 constant_dynamic-update-slice_fusion.5
  126.4 0.7 constant_dynamic-update-slice_fusion.4
  127.8 0.7 constant_dynamic-update-slice_fusion.2
  128.5 0.7 constant_dynamic-update-slice_fusion.1
  129.3 0.8 constant_dynamic-update-slice_fusion
  130.0 7.9 %fusion.3 = f32[1024,640]{1,0:T(8,128)} fusion(bf16[2048,1280]{1,0:T(8,128)(2,1)} %all-gather.2.cloned.1.call-done, bf16[1024,2048]{1,0:T(8,128)(2,1)} %param.5, f32[2048]{0:T(1024)S(1)} %convert_element_type.18, f32[1024]{0:T(1024)S(1)} %add_rsqrt_fusion), kind=kOutput, calls=%fused_computation.6 | convolution fusion | flops 2692743168 | bytes 9449472 | tf_op jit(solution)/shard_map/dot_general | solution.py:44
  138.0 13.1 %convolution_convert_fusion = bf16[1024,2048]{1,0:T(8,128)(2,1)} fusion(bf16[640,4096]{1,0:T(8,128)(2,1)} %constant_dynamic-update-slice_fusion, s32[]{:T(128)S(6)} %select_n.14, f32[1024,640]{1,0:T(8,128)} %fusion.3, bf16[2048,1280]{1,0:T(8,128)(2,1)} %all-gather.2.cloned.1.call-done, bf16[1024,2048]{1,0:T(8,128)(2,1)} %param.5, ...), kind=kOutput, calls=%fused_computation.5 | convolution fusion | flops 5383127040 | bytes 16265220 | tf_op jit(solution)/shard_map/dot_general | solution.py:47
  151.1 38.1 %reduce-scatter.2.cloned.1.call-done = bf16[128,2048]{1,0:T(8,128)(2,1)} async-done(((bf16[1024,2048]{1,0:T(8,128)(2,1)}), bf16[128,2048]{1,0:T(8,128)(2,1)}) %reduce-scatter.2.cloned.1.call-update) | async-done | bytes 524304 | tf_op jit(solution)/shard_map/reduce_scatter | solution.py:46
  (28 shorter events, 8.2 us)
Async XLA Ops:
  6.5 106.5 %copy-start = (bf16[640,128]{1,0:T(8,128)(2,1)S(1)}, bf16[640,128]{1,0:T(8,128)(2,1)}, u32[]{:S(2)}) copy-start(bf16[640,128]{1,0:T(8,128)(2,1)} %param.9) | copy-start | bytes 491524
  6.5 123.5 %all-gather.2.cloned.1.call-start = ((), (), s32[]{:S(2)}) async-start(), calls=%async_computation.1 | async-start | bytes 5570560 | tf_op jit(solution)/shard_map/all_gather | solution.py:25
  8.4 180.9 %reduce-scatter.2.cloned.1.call-start = ((), (), s32[]{:S(2)}) async-start(), calls=%async_computation.2 | async-start | bytes 4718592 | tf_op jit(solution)/shard_map/reduce_scatter | solution.py:46
  8.5 27.0 %collective-permute-start = (bf16[640,128]{1,0:T(8,128)(2,1)}, bf16[640,128]{1,0:T(8,128)(2,1)S(1)}, u32[]{:S(2)}, u32[]{:S(2)}) collective-permute-start(bf16[640,128]{1,0:T(8,128)(2,1)} %param.9), channel_id=1, source_target_pairs={{0,8},{8,16},{16,24},{24,32},{32,40},{40,48},{48,56},{56,64},{64,7... | collective-permute-start | bytes 491528 | tf_op jit(solution)/shard_map/ppermute | solution.py:15
  35.5 8.2 %collective-permute-start.1 = (bf16[640,128]{1,0:T(8,128)(2,1)S(1)}, bf16[640,128]{1,0:T(8,128)(2,1)S(1)}, u32[]{:S(2)}, u32[]{:S(2)}) collective-permute-start(bf16[640,128]{1,0:T(8,128)(2,1)S(1)} %collective-permute-done), channel_id=1, source_target_pairs={{0,8},{8,16},{16,24},{24,32},{32,40},{40,48},{48,56},{56,64},{64,7... | collective-permute-start | bytes 491528 | tf_op jit(solution)/shard_map/ppermute | solution.py:15
  35.5 9.5 %collective-permute-start.8 = (bf16[640,128]{1,0:T(8,128)(2,1)}, bf16[640,128]{1,0:T(8,128)(2,1)S(1)}, u32[]{:S(2)}, u32[]{:S(2)}) collective-permute-start(bf16[640,128]{1,0:T(8,128)(2,1)} %param.9), channel_id=1, source_target_pairs={{0,120},{8,0},{16,8},{24,16},{32,24},{40,32},{48,40},{56,48},{64,5... | collective-permute-start | bytes 491528 | tf_op jit(solution)/shard_map/ppermute | solution.py:17
  43.7 10.5 %collective-permute-start.2 = (bf16[640,128]{1,0:T(8,128)(2,1)S(1)}, bf16[640,128]{1,0:T(8,128)(2,1)S(1)}, u32[]{:S(2)}, u32[]{:S(2)}) collective-permute-start(bf16[640,128]{1,0:T(8,128)(2,1)S(1)} %collective-permute-done.1), channel_id=1, source_target_pairs={{0,8},{8,16},{16,24},{24,32},{32,40},{40,48},{48,56},{56,64},{64,7... | collective-permute-start | bytes 491528 | tf_op jit(solution)/shard_map/ppermute | solution.py:15
  45.0 10.3 %collective-permute-start.9 = (bf16[640,128]{1,0:T(8,128)(2,1)S(1)}, bf16[640,128]{1,0:T(8,128)(2,1)S(1)}, u32[]{:S(2)}, u32[]{:S(2)}) collective-permute-start(bf16[640,128]{1,0:T(8,128)(2,1)S(1)} %collective-permute-done.8), channel_id=1, source_target_pairs={{0,120},{8,0},{16,8},{24,16},{32,24},{40,32},{48,40},{56,48},{64,5... | collective-permute-start | bytes 491528 | tf_op jit(solution)/shard_map/ppermute | solution.py:17
  54.2 10.5 %collective-permute-start.3 = (bf16[640,128]{1,0:T(8,128)(2,1)S(1)}, bf16[640,128]{1,0:T(8,128)(2,1)S(1)}, u32[]{:S(2)}, u32[]{:S(2)}) collective-permute-start(bf16[640,128]{1,0:T(8,128)(2,1)S(1)} %collective-permute-done.2), channel_id=1, source_target_pairs={{0,8},{8,16},{16,24},{24,32},{32,40},{40,48},{48,56},{56,64},{64,7... | collective-permute-start | bytes 491528 | tf_op jit(solution)/shard_map/ppermute | solution.py:15
  55.3 10.4 %collective-permute-start.10 = (bf16[640,128]{1,0:T(8,128)(2,1)S(1)}, bf16[640,128]{1,0:T(8,128)(2,1)S(1)}, u32[]{:S(2)}, u32[]{:S(2)}) collective-permute-start(bf16[640,128]{1,0:T(8,128)(2,1)S(1)} %collective-permute-done.9), channel_id=1, source_target_pairs={{0,120},{8,0},{16,8},{24,16},{32,24},{40,32},{48,40},{56,48},{64,5... | collective-permute-start | bytes 491528 | tf_op jit(solution)/shard_map/ppermute | solution.py:17
  64.6 10.7 %collective-permute-start.4 = (bf16[640,128]{1,0:T(8,128)(2,1)S(1)}, bf16[640,128]{1,0:T(8,128)(2,1)S(1)}, u32[]{:S(2)}, u32[]{:S(2)}) collective-permute-start(bf16[640,128]{1,0:T(8,128)(2,1)S(1)} %collective-permute-done.3), channel_id=1, source_target_pairs={{0,8},{8,16},{16,24},{24,32},{32,40},{40,48},{48,56},{56,64},{64,7... | collective-permute-start | bytes 491528 | tf_op jit(solution)/shard_map/ppermute | solution.py:15
  65.7 10.2 %collective-permute-start.11 = (bf16[640,128]{1,0:T(8,128)(2,1)S(1)}, bf16[640,128]{1,0:T(8,128)(2,1)S(1)}, u32[]{:S(2)}, u32[]{:S(2)}) collective-permute-start(bf16[640,128]{1,0:T(8,128)(2,1)S(1)} %collective-permute-done.10), channel_id=1, source_target_pairs={{0,120},{8,0},{16,8},{24,16},{32,24},{40,32},{48,40},{56,48},{64,5... | collective-permute-start | bytes 491528 | tf_op jit(solution)/shard_map/ppermute | solution.py:17
  75.3 10.9 %collective-permute-start.5 = (bf16[640,128]{1,0:T(8,128)(2,1)S(1)}, bf16[640,128]{1,0:T(8,128)(2,1)S(1)}, u32[]{:S(2)}, u32[]{:S(2)}) collective-permute-start(bf16[640,128]{1,0:T(8,128)(2,1)S(1)} %collective-permute-done.4), channel_id=1, source_target_pairs={{0,8},{8,16},{16,24},{24,32},{32,40},{40,48},{48,56},{56,64},{64,7... | collective-permute-start | bytes 491528 | tf_op jit(solution)/shard_map/ppermute | solution.py:15
  75.8 14.2 %collective-permute-start.12 = (bf16[640,128]{1,0:T(8,128)(2,1)S(1)}, bf16[640,128]{1,0:T(8,128)(2,1)S(1)}, u32[]{:S(2)}, u32[]{:S(2)}) collective-permute-start(bf16[640,128]{1,0:T(8,128)(2,1)S(1)} %collective-permute-done.11), channel_id=1, source_target_pairs={{0,120},{8,0},{16,8},{24,16},{32,24},{40,32},{48,40},{56,48},{64,5... | collective-permute-start | bytes 491528 | tf_op jit(solution)/shard_map/ppermute | solution.py:17
  86.2 11.2 %collective-permute-start.6 = (bf16[640,128]{1,0:T(8,128)(2,1)S(1)}, bf16[640,128]{1,0:T(8,128)(2,1)S(1)}, u32[]{:S(2)}, u32[]{:S(2)}) collective-permute-start(bf16[640,128]{1,0:T(8,128)(2,1)S(1)} %collective-permute-done.5), channel_id=1, source_target_pairs={{0,8},{8,16},{16,24},{24,32},{32,40},{40,48},{48,56},{56,64},{64,7... | collective-permute-start | bytes 491528 | tf_op jit(solution)/shard_map/ppermute | solution.py:15
  90.0 10.6 %collective-permute-start.13 = (bf16[640,128]{1,0:T(8,128)(2,1)S(1)}, bf16[640,128]{1,0:T(8,128)(2,1)S(1)}, u32[]{:S(2)}, u32[]{:S(2)}) collective-permute-start(bf16[640,128]{1,0:T(8,128)(2,1)S(1)} %collective-permute-done.12), channel_id=1, source_target_pairs={{0,120},{8,0},{16,8},{24,16},{32,24},{40,32},{48,40},{56,48},{64,5... | collective-permute-start | bytes 491528 | tf_op jit(solution)/shard_map/ppermute | solution.py:17
  97.5 9.9 %collective-permute-start.7 = (bf16[640,128]{1,0:T(8,128)(2,1)S(1)}, bf16[640,128]{1,0:T(8,128)(2,1)S(1)}, u32[]{:S(2)}, u32[]{:S(2)}) collective-permute-start(bf16[640,128]{1,0:T(8,128)(2,1)S(1)} %collective-permute-done.6), channel_id=1, source_target_pairs={{0,8},{8,16},{16,24},{24,32},{32,40},{40,48},{48,56},{56,64},{64,7... | collective-permute-start | bytes 491528 | tf_op jit(solution)/shard_map/ppermute | solution.py:15
  100.6 17.3 %collective-permute-start.14 = (bf16[640,128]{1,0:T(8,128)(2,1)S(1)}, bf16[640,128]{1,0:T(8,128)(2,1)S(1)}, u32[]{:S(2)}, u32[]{:S(2)}) collective-permute-start(bf16[640,128]{1,0:T(8,128)(2,1)S(1)} %collective-permute-done.13), channel_id=1, source_target_pairs={{0,120},{8,0},{16,8},{24,16},{32,24},{40,32},{48,40},{56,48},{64,5... | collective-permute-start | bytes 491528 | tf_op jit(solution)/shard_map/ppermute | solution.py:17
Sparse Core Ops, SparseCore 0:
  9.1 108.8 all-gather.1
  151.3 37.9 reduce-scatter.1
